TPU v7x, 32 devices: a whole 2x2x4 slice. The times are simulated.
32 devices in a mesh: fs: 4 (over z), rep: 4 (over y, x), tp: 2 (over core).
Axes of the slice: x: 2, y: 2, z: 4, core: 2. Of those that a mesh axis runs over, the one named last changes fastest.
Arguments:
- saved_in: bfloat16 [4096, 4096], P(('fs', 'rep', 'tp')), may hold values from -6 to 6
- out_cot: bfloat16 [4096, 4096], P(('fs', 'rep', 'tp')), may hold values from -0.09375 to 0.09375
- value_cot: bfloat16 [4096, 2048], P(('fs', 'rep'), 'tp'), may hold values from -0.09375 to 0.09375
- mixed_out: bfloat16 [4096, 2048], P(('fs', 'rep'), 'tp'), may hold values from -6 to 6
- value_factor: bfloat16 [4096, 512], P('fs'), may hold values from -0.09375 to 0.09375
- out_factor: bfloat16 [4096, 512], P('fs'), may hold values from -0.09375 to 0.09375
- value_weight: float32 [4096, 2048], P('fs', 'tp'), may hold values from -0.09375 to 0.09375
- out_weight: float32 [2048, 4096], P('tp', 'fs'), may hold values from -0.125 to 0.125
- value_first: float32 [512, 2048], P('fs', 'tp'), may hold values from -6 to 6
- value_second: float32 [512, 2048], P('fs', 'tp'), may hold values from 0.25 to 4
- out_first: float32 [512, 2048], P('fs', 'tp'), may hold values from -6 to 6
- out_second: float32 [512, 2048], P('fs', 'tp'), may hold values from 0.25 to 4
Outputs:
- value_weight_new: float32 [4096, 2048], P('fs', 'tp')
- value_weight_copy: bfloat16 [4096, 2048], P('fs', 'tp')
- out_weight_new: float32 [2048, 4096], P('tp', 'fs')
- out_weight_copy: bfloat16 [2048, 4096], P('tp', 'fs')
- value_first_new: float32 [512, 2048], P('fs', 'tp')
- value_second_new: float32 [512, 2048], P('fs', 'tp')
- out_first_new: float32 [512, 2048], P('fs', 'tp')
- out_second_new: float32 [512, 2048], P('fs', 'tp')
- value_step: float32 [512, 2048], P('fs', 'tp')
- out_step: float32 [512, 2048], P('fs', 'tp')
All inputs are finite; a program needn't handle non-finite values.
Results may differ from a plain program's by a relative error of at most 0.005.
Values may be sent and summed in bfloat16 or wider, within the bound.
A program may use at most 128 MiB of HBM per device.

v0:
```python
import jax
import jax.numpy as jnp
from jax import lax
from jax.sharding import PartitionSpec as P

CHANNELS = 2048
RANK = 512


beta_first = 0.8
beta_second = 0.9
step_rate = 0.05
clip_level = 0.5


def fold_pair(left_in, left_cot, pieces):
    return (
        jnp.dot(left_in, pieces[0], preferred_element_type=jnp.float32),
        jnp.dot(left_cot, pieces[1], preferred_element_type=jnp.float32),
    )


def contract_rows(left, right):
    return lax.dot_general(
        left, right, (((0,), (0,)), ((), ())), preferred_element_type=jnp.float32
    )


def adapt(grad, first, second):
    new_first = beta_first * first + (1.0 - beta_first) * grad
    new_second = beta_second * second + (1.0 - beta_second) * grad * grad
    lowered = (new_first / jnp.sqrt(new_second)).astype(jnp.bfloat16)
    return (new_first, new_second, lowered)


def shards(
    saved_in,
    out_cot,
    value_cot,
    mixed_out,
    value_factor,
    out_factor,
    value_weight,
    out_weight,
    value_first,
    value_second,
    out_first,
    out_second,
):
    rank_cols = value_factor.shape[1]
    half_width = rank_cols // 2
    offset = lax.axis_index("tp") * half_width
    half_value = lax.dynamic_slice_in_dim(value_factor, offset, half_width, 1)
    half_out = lax.dynamic_slice_in_dim(out_factor, offset, half_width, 1)
    both_in, both_cot = (
        lax.all_gather(saved_in, "tp", axis=0, tiled=True),
        lax.all_gather(out_cot, "tp", axis=0, tiled=True),
    )
    proj_in, proj_cot = fold_pair(
        both_in,
        both_cot,
        (
            lax.all_gather(half_value, "fs", axis=0, tiled=True),
            lax.all_gather(half_out, "fs", axis=0, tiled=True),
        ),
    )
    proj_in, proj_cot = (
        lax.all_gather(proj_in.astype(jnp.bfloat16), "tp", axis=1, tiled=True),
        lax.all_gather(proj_cot.astype(jnp.bfloat16), "tp", axis=1, tiled=True),
    )
    summed = lax.psum_scatter(
        jnp.concatenate(
            [contract_rows(proj_in, value_cot), contract_rows(proj_cot, mixed_out)], axis=1
        ),
        "fs",
        scatter_dimension=0,
        tiled=True,
    )
    summed = lax.psum(summed.astype(jnp.bfloat16), "rep").astype(jnp.float32)
    chan_cols = value_cot.shape[1]
    value_first_new, value_second_new, low_value = adapt(
        summed[:, :chan_cols], value_first, value_second
    )
    out_first_new, out_second_new, low_out = adapt(summed[:, chan_cols:], out_first, out_second)
    lowered = jnp.concatenate([low_value, low_out], axis=1)
    gathered = lax.all_gather(lowered, "fs", axis=0, tiled=True)
    own_float = lowered.astype(jnp.float32)
    total = lax.psum(jnp.sum(own_float * own_float), ("fs", "tp"))
    spread = jnp.sqrt(total / (2.0 * RANK * CHANNELS))
    scale = clip_level / jnp.maximum(spread, clip_level)
    value_full = jnp.dot(value_factor, gathered[:, :chan_cols], preferred_element_type=jnp.float32)
    out_full = lax.dot_general(
        gathered[:, chan_cols:],
        out_factor,
        (((0,), (1,)), ((), ())),
        preferred_element_type=jnp.float32,
    )
    value_weight_new = value_weight - step_rate * scale * value_full
    out_weight_new = out_weight - step_rate * scale * out_full
    return (
        value_weight_new,
        value_weight_new.astype(jnp.bfloat16),
        out_weight_new,
        out_weight_new.astype(jnp.bfloat16),
        value_first_new,
        value_second_new,
        out_first_new,
        out_second_new,
        scale * low_value.astype(jnp.float32),
        scale * low_out.astype(jnp.float32),
    )


def solution(mesh):
    placed = (
        P(("fs", "rep", "tp"), None),
        P(("fs", "rep", "tp"), None),
        P(("fs", "rep"), "tp"),
        P(("fs", "rep"), "tp"),
        P("fs", None),
        P("fs", None),
        P("fs", "tp"),
        P("tp", "fs"),
        P("fs", "tp"),
        P("fs", "tp"),
        P("fs", "tp"),
        P("fs", "tp"),
    )
    return jax.shard_map(
        shards,
        mesh=mesh,
        in_specs=placed,
        out_specs=(
            P("fs", "tp"),
            P("fs", "tp"),
            P("tp", "fs"),
            P("tp", "fs"),
            P("fs", "tp"),
            P("fs", "tp"),
            P("fs", "tp"),
            P("fs", "tp"),
            P("fs", "tp"),
            P("fs", "tp"),
        ),
        check_vma=False,
    )
```

profile of v0, /device:TPU:0, one launch (start us, length us, event | category | flops | bytes accessed | tf_op | source)
XLA Modules:
  0.0 343.5 jit_solution(9463912163922284512)
XLA Ops:
  7.2 0.0 copy-start
  7.2 0.0 all-gather.12.cloned.1.call-start
  7.2 0.7 all-gather.12.cloned.1.call-update
  7.9 0.0 all-gather.10.cloned.1.call-start
  8.0 1.9 constant_dynamic-slice_fusion
  9.9 0.0 all-gather.10.cloned.1.call-update
  9.9 0.0 all-gather.8.cloned.1.call-start
  9.9 0.7 all-gather.8.cloned.1.call-update
  10.6 0.0 all-gather.6.cloned.1.call-start
  10.7 0.8 constant_dynamic-slice_fusion.1
  11.5 0.0 all-gather.6.cloned.1.call-update
  11.5 0.0 reduce-scatter.2.cloned.1.call-start
  11.6 11.3 %all-gather.12.cloned.1.call-done = bf16[256,4096]{1,0:T(8,128)(2,1)} async-done(((bf16[128,4096]{1,0:T(8,128)(2,1)}), bf16[256,4096]{1,0:T(8,128)(2,1)}) %all-gather.12.cloned.1.call-update) | async-done | bytes 2097168 | tf_op jit(solution)/shard_map/all_gather | solution.py:57
  22.9 49.0 %all-gather.10.cloned.1.call-done = bf16[4096,256]{1,0:T(8,128)(2,1)} async-done(((bf16[1024,256]{1,0:T(8,128)(2,1)}), bf16[4096,256]{1,0:T(8,128)(2,1)}) %all-gather.10.cloned.1.call-update) | async-done | bytes 2097168 | tf_op jit(solution)/shard_map/all_gather | solution.py:64
  71.9 3.0 fusion.1
  74.9 2.0 all_gather.26
  76.9 6.0 %all-gather.8.cloned.1.call-done = bf16[256,4096]{1,0:T(8,128)(2,1)} async-done(((bf16[128,4096]{1,0:T(8,128)(2,1)}), bf16[256,4096]{1,0:T(8,128)(2,1)}) %all-gather.8.cloned.1.call-update) | async-done | bytes 2097168 | tf_op jit(solution)/shard_map/all_gather | solution.py:56
  82.8 48.9 %all-gather.6.cloned.1.call-done = bf16[4096,256]{1,0:T(8,128)(2,1)} async-done(((bf16[1024,256]{1,0:T(8,128)(2,1)}), bf16[4096,256]{1,0:T(8,128)(2,1)}) %all-gather.6.cloned.1.call-update) | async-done | bytes 2097168 | tf_op jit(solution)/shard_map/all_gather | solution.py:63
  131.7 3.0 fusion
  134.7 0.0 copy-start.2
  134.7 2.1 all_gather.23
  136.8 0.4 fusion.11
  137.3 0.4 fusion.10
  137.7 2.5 pad_maximum_fusion
  140.2 0.0 reduce-scatter.2.cloned.1.call-update
  140.3 0.0 copy-start.3
  140.3 0.0 copy-start.4
  140.3 0.0 copy-start.5
  140.3 0.0 all-reduce.2.cloned.1.call-start
  140.3 75.7 %reduce-scatter.2.cloned.1.call-done = f32[128,2048]{1,0:T(8,128)} async-done(((f32[512,2048]{1,0:T(8,128)}), f32[128,2048]{1,0:T(8,128)}) %reduce-scatter.2.cloned.1.call-update) | async-done | bytes 1048592 | tf_op jit(solution)/shard_map/reduce_scatter | solution.py:71
  216.0 2.1 convert_element_type.43
  218.1 0.0 all-reduce.2.cloned.1.call-update
  218.1 0.0 all-gather.14.cloned.1.call-start
  218.2 47.2 %all-reduce.2.cloned.1.call-done = bf16[128,2048]{1,0:T(8,128)(2,1)} async-done(((bf16[128,2048]{1,0:T(8,128)(2,1)}), bf16[128,2048]{1,0:T(8,128)(2,1)}) %all-reduce.2.cloned.1.call-update) | async-done | bytes 524304 | tf_op jit(solution)/shard_map/psum | solution.py:79
  265.3 1.1 convert_element_type.44
  266.5 0.0 copy-done.3
  266.5 2.6 multiply_convert_fusion.1
  269.1 0.8 pad_maximum_fusion.1
  270.0 0.0 all-gather.14.cloned.1.call-update
  270.0 0.9 multiply_reduce_fusion
  270.9 5.3 %copy.22 = f32[1024,1024]{0,1:T(8,128)} copy(f32[1024,1024]{1,0:T(8,128)} %param.18) | data formatting | bytes 8388608 | tf_op args[6]
  276.2 17.6 %psum.15 = f32[]{:T(128)} all-reduce(f32[]{:T(128)} %multiply_reduce_fusion), channel_id=1, replica_groups=mesh['fs'=4,'rep'=4,'tp'=2] {'fs','tp'}, use_global_device_ids=true, to_apply=%region_3.0 | all-reduce | flops 1 | bytes 8 | tf_op jit(solution)/shard_map/psum | solution.py:88
  294.6 1.1 convert_multiply_fusion
  295.7 20.4 %all-gather.14.cloned.1.call-done = bf16[512,2048]{1,0:T(8,128)(2,1)} async-done(((bf16[128,2048]{1,0:T(8,128)(2,1)}), bf16[512,2048]{1,0:T(8,128)(2,1)}) %all-gather.14.cloned.1.call-update) | async-done | bytes 2097168 | tf_op jit(solution)/shard_map/all_gather | solution.py:86
  316.1 5.8 %fusion.8 = (bf16[1024,1024]{0,1:T(8,128)(2,1)S(1)}, f32[1024,1024]{0,1:T(8,128)}) fusion(f32[1024,1024]{0,1:T(8,128)} %copy.22, bf16[1024,512]{1,0:T(8,128)(2,1)S(1)} %copy-done, bf16[512,2048]{1,0:T(8,128)(2,1)} %all-gather.14.cloned.1.call-done, f32[]{:T(128)S(6)} %mul.75), kind=kOutput, calls=%fused_computation.23 | convolution fusion | flops 1076887552 | bytes 12582916 | tf_op jit(solution)/shard_map/dot_general | solution.py:91
  321.9 5.3 %copy.23 = f32[1024,1024]{1,0:T(8,128)} copy(f32[1024,1024]{0,1:T(8,128)} %get-tuple-element.30) | data formatting | bytes 8388608
  327.3 2.5 copy.24
  329.8 6.8 %fusion.9 = (bf16[1024,1024]{1,0:T(8,128)(2,1)}, f32[1024,1024]{1,0:T(8,128)}) fusion(f32[1024,1024]{1,0:T(8,128)} %param.19, bf16[1024,512]{1,0:T(8,128)(2,1)} %param.17, bf16[512,2048]{1,0:T(8,128)(2,1)} %all-gather.14.cloned.1.call-done, f32[]{:T(128)S(6)} %mul.75), kind=kOutput, calls=%fused_computation.24 | convolution fusion | flops 1076887552 | bytes 12582916 | tf_op jit(solution)/shard_map/dot_general | solution.py:92
  (6 shorter events, 0.0 us)
Async XLA Ops:
  7.2 3.5 %copy-start = (bf16[1024,512]{1,0:T(8,128)(2,1)S(1)}, bf16[1024,512]{1,0:T(8,128)(2,1)}, u32[]{:S(2)}) copy-start(bf16[1024,512]{1,0:T(8,128)(2,1)} %param.16) | copy-start | bytes 3145732
  7.2 15.7 %all-gather.12.cloned.1.call-start = ((), (), s32[]{:S(2)}) async-start(), calls=%async_computation.4 | async-start | bytes 3145728 | tf_op jit(solution)/shard_map/all_gather | solution.py:57
  7.9 64.0 %all-gather.10.cloned.1.call-start = ((), (), s32[]{:S(2)}) async-start(), calls=%async_computation.3 | async-start | bytes 2621440 | tf_op jit(solution)/shard_map/all_gather | solution.py:64
  9.9 73.0 %all-gather.8.cloned.1.call-start = ((), (), s32[]{:S(2)}) async-start(), calls=%async_computation.2 | async-start | bytes 3145728 | tf_op jit(solution)/shard_map/all_gather | solution.py:56
  10.6 121.1 %all-gather.6.cloned.1.call-start = ((), (), s32[]{:S(2)}) async-start(), calls=%async_computation.1 | async-start | bytes 2621440 | tf_op jit(solution)/shard_map/all_gather | solution.py:63
  11.5 204.5 %reduce-scatter.2.cloned.1.call-start = ((), (), s32[]{:S(2)}) async-start(), calls=%async_computation.5 | async-start | bytes 5242880 | tf_op jit(solution)/shard_map/reduce_scatter | solution.py:71
  76.9 60.0 %copy-start.1 = (bf16[256,1024]{1,0:T(8,128)(2,1)S(1)}, bf16[256,1024]{1,0:T(8,128)(2,1)}, u32[]{:S(2)}) copy-start(bf16[256,1024]{1,0:T(8,128)(2,1)} %param.15) | copy-start | bytes 1572868
  134.7 2.6 copy-start.2
  140.3 126.2 %copy-start.3 = (f32[128,1024]{1,0:T(8,128)S(1)}, f32[128,1024]{1,0:T(8,128)}, u32[]{:S(2)}) copy-start(f32[128,1024]{1,0:T(8,128)} %param.21) | copy-start | bytes 1572868
  140.3 126.2 %copy-start.4 = (f32[128,1024]{1,0:T(8,128)S(1)}, f32[128,1024]{1,0:T(8,128)}, u32[]{:S(2)}) copy-start(f32[128,1024]{1,0:T(8,128)} %param.20) | copy-start | bytes 1572868
  140.3 126.2 %copy-start.5 = (f32[128,1024]{1,0:T(8,128)S(1)}, f32[128,1024]{1,0:T(8,128)}, u32[]{:S(2)}) copy-start(f32[128,1024]{1,0:T(8,128)} %param.23) | copy-start | bytes 1572868
  140.3 125.0 %all-reduce.2.cloned.1.call-start = ((), (), s32[]{:S(2)}) async-start(), calls=%async_computation.6 | async-start | bytes 1048576 | tf_op jit(solution)/shard_map/psum | solution.py:79
  218.1 98.0 %all-gather.14.cloned.1.call-start = ((), (), s32[]{:S(2)}) async-start(), calls=%async_computation.7 | async-start | bytes 2621440 | tf_op jit(solution)/shard_map/all_gather | solution.py:86
Sparse Core Ops, SparseCore 0:
  9.5 13.2 all-gather.11
  25.0 46.8 all-gather.9
  73.4 9.3 all-gather.7
  84.8 46.8 all-gather.5
  140.4 75.5 reduce-scatter.1
  219.4 45.8 all-reduce.1
  270.1 45.9 all-gather.13
where the time goes:
time: 344 us; the launch traced here: 343 us
  waiting for transfers between devices  260 us (76%)
  blocking collectives  21.8 us (6%)
  matrix products  19.5 us (6%)
  local copies, waits for them, and re-layouts  16 us (5%)
  between operations  15 us (4%)
  other arithmetic  11.1 us (3%)
    reduce_scatter x1, waiting for transfers between devices, shards(): lax.psum_scatter(jnp.concatenate([contract_rows(proj_in, value_cot), cont...  75.7 us
    all_gather x1, waiting for transfers between devices, shards(): lax.all_gather(half_out, 'fs', axis=0, tiled=True)  49 us
    all_gather x1, waiting for transfers between devices, shards(): lax.all_gather(half_value, 'fs', axis=0, tiled=True)  48.9 us
    psum x1, waiting for transfers between devices, shards(): summed = lax.psum(summed.astype(jnp.bfloat16), 'rep').astype(jnp.float32)  47.2 us
    all_gather x1, waiting for transfers between devices, shards(): gathered = lax.all_gather(lowered, 'fs', axis=0, tiled=True)  20.4 us
    psum x1, blocking collectives, shards(): total = lax.psum(jnp.sum(own_float * own_float), ('fs', 'tp'))  17.6 us
    unnamed x15, local copies, waits for them, and re-layouts  13.3 us
    all_gather x1, waiting for transfers between devices, shards(): lax.all_gather(out_cot, 'tp', axis=0, tiled=True)  11.3 us
  transfers between devices with their start and end apart: 7, of which 7 were waited for; matrix products, arithmetic and copies ran while one was open for 4% of the time, Pallas kernels for 0%

commit v1 on v0

v1 whole, which is shorter than its diff:
```python
import functools

import jax
import jax.numpy as jnp
from jax import lax
from jax.experimental import pallas as pl
from jax.experimental.pallas import tpu as pltpu
from jax.sharding import PartitionSpec as P

beta_first = 0.8
beta_second = 0.9
step_rate = 0.05
clip_level = 0.5
MESH = pl.DeviceIdType.MESH
F32 = jnp.float32
BF16 = jnp.bfloat16


def blend(grad, first, second):
    new_first = beta_first * first + (1.0 - beta_first) * grad
    new_second = beta_second * second + (1.0 - beta_second) * grad * grad
    return new_first, new_second


def exchange_kernel(
    nfs, nrep,
    xs0, xs1, ct0, ct1, fa0, fa1, m10, m20, m11, m21,
    low0, low1, grad0, grad1, tot_out,
    xin0, xin1, fb0, fb1, cv0, cv1, pb0, pb1, pt0, pt1, ra0, ra1, s0, s1, rb0, rb1,
    gb0, gb1, lb0, lb1, mo, tb, acc,
    lsem, xsem, zsem, bsem, csem, asem, rsem, gsem, lzsem, lxsem, tsem, osem,
):
    j = lax.axis_index("fs")
    r = lax.axis_index("rep")
    c = lax.axis_index("tp")
    mate = 1 - c
    xs, ct, fa, firsts, seconds = (xs0, xs1), (ct0, ct1), (fa0, fa1), (m10, m11), (m20, m21)
    lows, grads = (low0, low1), (grad0, grad1)
    xin, fb, cv, pb, pt, ra, sm, rb = (
        (xin0, xin1), (fb0, fb1), (cv0, cv1), (pb0, pb1), (pt0, pt1), (ra0, ra1), (s0, s1), (rb0, rb1),
    )
    gb, lb = (gb0, gb1), (lb0, lb1)
    rows = xs0.shape[0]
    depth, half = fb0.shape
    block = depth // nfs
    quarter = block // nrep
    chunk, width = rb0.shape[1:]
    zd = range(1, nfs)
    xd = range(1, nrep)

    def fs_at(d):
        return lax.rem(j + d + nfs, nfs)

    def rep_at(e):
        return lax.rem(r + e + nrep, nrep)

    def remote(src, dst, sems, idx, where):
        return pltpu.make_async_remote_copy(
            src_ref=src, dst_ref=dst, send_sem=sems.at[(0, *idx)], recv_sem=sems.at[(1, *idx)],
            device_id=where, device_id_type=MESH,
        )

    mine = pl.ds(pl.multiple_of(c * rows, rows), rows)
    half_cols = pl.ds(pl.multiple_of(c * half, half), half)
    own_rows = pl.ds(pl.multiple_of(j * block, block), block)
    mcols = pl.ds(pl.multiple_of(r * width, width), width)
    local = {}
    for f in (0, 1):
        local["x", f] = pltpu.make_async_copy(xs[f], xin[f].at[mine], lsem.at[0, f])
        local["f", f] = pltpu.make_async_copy(fa[f].at[:, half_cols], fb[f].at[own_rows], lsem.at[1, f])
        local["c", f] = pltpu.make_async_copy(ct[f], cv[f], lsem.at[2, f])
        local["1", f] = pltpu.make_async_copy(firsts[f].at[:, mcols], mo.at[f, 0], lsem.at[3, f])
        local["2", f] = pltpu.make_async_copy(seconds[f].at[:, mcols], mo.at[f, 1], lsem.at[4, f])

    barrier = pltpu.get_barrier_semaphore()
    for d in zd:
        pl.semaphore_signal(barrier, inc=1, device_id={"fs": fs_at(d)}, device_id_type=MESH)
    for e in xd:
        pl.semaphore_signal(barrier, inc=1, device_id={"rep": rep_at(e)}, device_id_type=MESH)
    pl.semaphore_signal(barrier, inc=1, device_id={"tp": mate}, device_id_type=MESH)
    for f in (0, 1):
        for k in ("x", "f", "c", "1", "2"):
            local[k, f].start()
    pl.semaphore_wait(barrier, nfs + nrep - 1)

    def frows(jj, rr):
        return pl.ds(pl.multiple_of(jj * block + rr * quarter, quarter), quarter)

    sends = []
    zcp = {}
    for f in (0, 1):
        for d in zd:
            cp = remote(
                fa[f].at[pl.ds(pl.multiple_of(r * quarter, quarter), quarter), half_cols],
                fb[f].at[frows(j, r)], zsem, (f, d - 1), {"fs": fs_at(d)},
            )
            cp.start()
            sends.append(cp)
            zcp[f, d] = remote(
                fa[f].at[pl.ds(pl.multiple_of(r * quarter, quarter), quarter), half_cols],
                fb[f].at[frows(fs_at(-d), r)], zsem, (f, d - 1), {"fs": fs_at(d)},
            )
    xcp = []
    for f in (0, 1):
        cp = remote(xs[f], xin[f].at[mine], xsem, (f,), {"tp": mate})
        cp.start()
        sends.append(cp)
        theirs = pl.ds(pl.multiple_of(mate * rows, rows), rows)
        xcp.append(remote(xs[f], xin[f].at[theirs], xsem, (f,), {"tp": mate}))
    for f in (0, 1):
        for d in zd:
            zcp[f, d].wait_recv()
            for e in xd:
                view = fb[f].at[frows(fs_at(-d), r)]
                cp = remote(view, view, bsem, (f, d - 1, e - 1), {"rep": rep_at(e)})
                cp.start()
                sends.append(cp)

    kstep = min(512, depth)
    perhalf = half // chunk

    for f in (0, 1):
        for k in ("x", "f", "c"):
            local[k, f].wait()
        xcp[f].wait_recv()
        for d in zd:
            for e in xd:
                view = fb[f].at[frows(fs_at(-d), rep_at(-e))]
                remote(view, view, bsem, (f, d - 1, e - 1), {"rep": rep_at(e)}).wait_recv()

        acc[...] = jnp.zeros_like(acc)

        def project(k, _, f=f):
            ks = pl.ds(pl.multiple_of(k * kstep, kstep), kstep)
            acc[...] += jnp.dot(xin[f][:, ks], fb[f][ks, :], preferred_element_type=F32)
            return 0

        lax.fori_loop(0, depth // kstep, project, 0)
        pb[f][c] = jnp.transpose(acc[...]).astype(BF16)
        cp = remote(pb[f].at[c], pb[f].at[c], csem, (f,), {"tp": mate})
        cp.start()
        sends.append(cp)

        def partials(h, f=f):
            left = pb[f][h]

            def piece(q, _):
                cols = pl.ds(pl.multiple_of(q * width, width), width)
                out = jnp.dot(left, cv[f][:, cols], preferred_element_type=F32)
                for i in range(perhalf):
                    pt[f][q, h * perhalf + i] = out[i * chunk:(i + 1) * chunk].astype(BF16)
                return 0

            lax.fori_loop(0, nrep, piece, 0)

        partials(c)
        remote(pb[f].at[mate], pb[f].at[mate], csem, (f,), {"tp": mate}).wait_recv()
        partials(mate)
        for e in xd:
            cp = remote(pt[f].at[rep_at(e)], ra[f].at[e - 1], asem, (f, e - 1), {"rep": rep_at(e)})
            cp.start()
            sends.append(cp)

    for f in (0, 1):
        for e in xd:
            remote(pt[f].at[rep_at(e)], ra[f].at[e - 1], asem, (f, e - 1), {"rep": rep_at(e)}).wait_recv()

        def add(i, _, f=f):
            total = pt[f][r, i].astype(F32)
            for e in xd:
                total += ra[f][e - 1, i].astype(F32)
            sm[f][i] = total.astype(BF16)
            return 0

        lax.fori_loop(0, nfs, add, 0)
        for d in zd:
            cp = remote(sm[f].at[fs_at(d)], rb[f].at[d - 1], rsem, (f, d - 1), {"fs": fs_at(d)})
            cp.start()
            sends.append(cp)

    for f in (0, 1):
        local["1", f].wait()
        local["2", f].wait()
        for d in zd:
            remote(sm[f].at[fs_at(d)], rb[f].at[d - 1], rsem, (f, d - 1), {"fs": fs_at(d)}).wait_recv()
        total = sm[f][j].astype(F32)
        for d in zd:
            total += rb[f][d - 1].astype(F32)
        kept = total.astype(BF16)
        gb[f][r] = kept
        new_first, new_second = blend(kept.astype(F32), mo[f, 0], mo[f, 1])
        lb[f][r, j] = (new_first / jnp.sqrt(new_second)).astype(BF16)
        for d in zd:
            view = lb[f].at[r, j]
            cp = remote(view, view, lzsem, (f, d - 1), {"fs": fs_at(d)})
            cp.start()
            sends.append(cp)
        for e in xd:
            view = lb[f].at[r, j]
            cp = remote(view, view, lxsem, (f, 0, e - 1), {"rep": rep_at(e)})
            cp.start()
            sends.append(cp)

    for f in (0, 1):
        for d in zd:
            view = lb[f].at[r, fs_at(-d)]
            remote(view, view, lzsem, (f, d - 1), {"fs": fs_at(d)}).wait_recv()
            for e in xd:
                cp = remote(view, view, lxsem, (f, d, e - 1), {"rep": rep_at(e)})
                cp.start()
                sends.append(cp)
    for f in (0, 1):
        for e in xd:
            cp = remote(gb[f].at[r], gb[f].at[r], gsem, (f, e - 1), {"rep": rep_at(e)})
            cp.start()
            sends.append(cp)
    for f in (0, 1):
        for d in range(nfs):
            for e in xd:
                view = lb[f].at[rep_at(-e), fs_at(-d)]
                remote(view, view, lxsem, (f, d, e - 1), {"rep": rep_at(e)}).wait_recv()
    outs = []
    for f in (0, 1):
        cp = pltpu.make_async_copy(lb[f], lows[f], osem.at[f, 0])
        cp.start()
        outs.append(cp)

    zero = jnp.zeros((chunk, width), F32)

    def square(i, carry):
        q, k = i // nfs, i % nfs
        for f in (0, 1):
            part = lb[f][q, k].astype(F32)
            carry = carry + part * part
        return carry

    squares = jnp.sum(lax.fori_loop(0, nrep * nfs, square, zero))
    tb[c] = jnp.full(tb.shape[1:], squares, F32)
    cp = remote(tb.at[c], tb.at[c], tsem, (), {"tp": mate})
    cp.start()
    sends.append(cp)
    for f in (0, 1):
        for e in xd:
            view = gb[f].at[rep_at(-e)]
            remote(view, view, gsem, (f, e - 1), {"rep": rep_at(e)}).wait_recv()
        cp = pltpu.make_async_copy(gb[f], grads[f], osem.at[f, 1])
        cp.start()
        outs.append(cp)
    remote(tb.at[mate], tb.at[mate], tsem, (), {"tp": mate}).wait_recv()
    tot_out[...] = tb[0] + tb[1]
    for cp in outs:
        cp.wait()
    for cp in sends:
        cp.wait_send()


def update_kernel(
    count, tot, low0, low1, grad0, grad1, fa0, fa1, w0, w1, m10, m20, m11, m21,
    nw0, cw0, nw1, cw1, n10, n20, n11, n21, st0, st1,
):
    spread = jnp.sqrt(tot[0:1, 0:1] / count)
    scale = clip_level / jnp.maximum(spread, clip_level)
    for grad, m1, m2, n1, n2, st in (
        (grad0, m10, m20, n10, n20, st0), (grad1, m11, m21, n11, n21, st1),
    ):
        new_first, new_second = blend(grad[0].astype(F32), m1[...], m2[...])
        n1[...] = new_first
        n2[...] = new_second
        low = (new_first / jnp.sqrt(new_second)).astype(BF16)
        st[...] = scale * low.astype(F32)
    full = jnp.dot(fa0[...], low0[0], preferred_element_type=F32)
    new = w0[...] - step_rate * scale * full
    nw0[...] = new
    cw0[...] = new.astype(BF16)
    full = lax.dot_general(low1[0], fa1[...], (((0,), (1,)), ((), ())), preferred_element_type=F32)
    new = w1[...] - step_rate * scale * full
    nw1[...] = new
    cw1[...] = new.astype(BF16)


def shards(nfs, nrep, ntp, xs0, xs1, ct0, ct1, fa0, fa1, w0, w1, m10, m20, m11, m21):
    rows, depth = xs0.shape
    tokens, chans = ct0.shape
    rank = fa0.shape[1]
    half = rank // ntp
    chunk = rank // nfs
    width = chans // nrep
    hbm = pl.BlockSpec(memory_space=pl.ANY)
    vmem = pl.BlockSpec(memory_space=pltpu.VMEM)
    sds = jax.ShapeDtypeStruct

    def twice(shape, dtype=BF16):
        return [pltpu.VMEM(shape, dtype)] * 2

    def sems(*shape):
        return pltpu.SemaphoreType.DMA(shape)

    low0, low1, grad0, grad1, tot = pl.pallas_call(
        functools.partial(exchange_kernel, nfs, nrep),
        out_shape=[sds((nrep, nfs, chunk, width), BF16)] * 2
        + [sds((nrep, chunk, width), BF16)] * 2
        + [sds((8, 128), F32)],
        in_specs=[hbm] * 10,
        out_specs=[hbm] * 4 + [vmem],
        scratch_shapes=twice((tokens, depth))
        + twice((depth, half))
        + twice((tokens, chans))
        + twice((ntp, half, tokens))
        + twice((nrep, nfs, chunk, width))
        + twice((nrep - 1, nfs, chunk, width))
        + twice((nfs, chunk, width))
        + twice((nfs - 1, chunk, width))
        + twice((nrep, chunk, width))
        + twice((nrep, nfs, chunk, width))
        + [pltpu.VMEM((2, 2, chunk, width), F32), pltpu.VMEM((ntp, 8, 128), F32), pltpu.VMEM((tokens, half), F32)]
        + [
            sems(5, 2),
            sems(2, 2),
            sems(2, 2, nfs - 1),
            sems(2, 2, nfs - 1, nrep - 1),
            sems(2, 2),
            sems(2, 2, nrep - 1),
            sems(2, 2, nfs - 1),
            sems(2, 2, nrep - 1),
            sems(2, 2, nfs - 1),
            sems(2, 2, nfs, nrep - 1),
            sems(2),
            sems(2, 2),
        ],
        compiler_params=pltpu.CompilerParams(
            collective_id=0, has_side_effects=True, vmem_limit_bytes=48 * 1024 * 1024
        ),
        name="exchange",
    )(xs0, xs1, ct0, ct1, fa0, fa1, m10, m20, m11, m21)
    low0 = low0.reshape(nrep, rank, width)
    low1 = low1.reshape(nrep, rank, width)

    block = fa0.shape[0]
    one = pl.BlockSpec((1, rank, width), lambda q: (q, 0, 0))
    gsp = pl.BlockSpec((1, chunk, width), lambda q: (q, 0, 0))
    whole = pl.BlockSpec((block, rank), lambda q: (0, 0))
    wcol = pl.BlockSpec((block, width), lambda q: (0, q))
    wrow = pl.BlockSpec((width, block), lambda q: (q, 0))
    msp = pl.BlockSpec((chunk, width), lambda q: (0, q))
    moment = sds((chunk, chans), F32)
    nw0, cw0, nw1, cw1, n10, n20, n11, n21, st0, st1 = pl.pallas_call(
        functools.partial(update_kernel, 2.0 * rank * chans * ntp),
        grid=(nrep,),
        out_shape=[
            sds((block, chans), F32), sds((block, chans), BF16),
            sds((chans, block), F32), sds((chans, block), BF16),
        ] + [moment] * 6,
        in_specs=[pl.BlockSpec((8, 128), lambda q: (0, 0)), one, one, gsp, gsp, whole, whole, wcol, wrow]
        + [msp] * 4,
        out_specs=[wcol, wcol, wrow, wrow] + [msp] * 6,
        compiler_params=pltpu.CompilerParams(vmem_limit_bytes=48 * 1024 * 1024),
        name="update",
    )(tot, low0, low1, grad0, grad1, fa0, fa1, w0, w1, m10, m20, m11, m21)
    return nw0, cw0, nw1, cw1, n10, n20, n11, n21, st0, st1


def solution(mesh):
    tokens = P(("fs", "rep", "tp"), None)
    mixed = P(("fs", "rep"), "tp")
    factor = P("fs", None)
    plain = P("fs", "tp")
    flipped = P("tp", "fs")
    sizes = mesh.shape
    return jax.shard_map(
        functools.partial(shards, sizes["fs"], sizes["rep"], sizes["tp"]),
        mesh=mesh,
        in_specs=(tokens, tokens, mixed, mixed, factor, factor, plain, flipped, plain, plain, plain, plain),
        out_specs=(plain, plain, flipped, flipped, plain, plain, plain, plain, plain, plain),
        check_vma=False,
    )
```

time: 344 us -> 125 us (0.36)
  the two profiles are of different devices: /device:TPU:0 before, /device:TPU:16 now
where the time goes in v1:
time: 125 us
  Pallas kernels  118 us (94%)
  local copies, waits for them, and re-layouts  6.33 us (5%)
    pallas_call x1, Pallas kernels, shards(): pl.pallas_call(functools.partial(exchange_kernel, nfs, nrep), out_shape=[...  108 us
    pallas_call x1, Pallas kernels, shards(): pl.pallas_call(functools.partial(update_kernel, 2.0 * rank * chans * ntp)...  10.2 us
    unnamed x14, local copies, waits for them, and re-layouts  6.33 us

profile of v1, /device:TPU:16, one launch (start us, length us, event | category | flops | bytes accessed | tf_op | source)
XLA Modules:
  0.0 125.0 jit_solution(17537915185568849409)
XLA Ops:
  0.6 0.0 copy-start
  0.7 0.0 copy-start.1
  0.7 1.1 copy-done.1
  1.8 0.0 copy-start.2
  1.8 1.0 copy-done.2
  2.8 0.0 copy-start.3
  2.8 1.0 copy-done.3
  3.9 0.0 copy-start.4
  3.9 1.0 copy-done.4
  4.9 0.0 copy-start.5
  4.9 1.0 copy-done.5
  6.0 0.0 copy-start.6
  6.0 1.0 copy-done.6
  7.0 107.8 %exchange.1 = (bf16[4,4,128,256]{3,2,1,0:T(8,128)(2,1)S(1)}, bf16[4,4,128,256]{3,2,1,0:T(8,128)(2,1)S(1)}, bf16[4,128,256]{2,1,0:T(8,128)(2,1)S(1)}, bf16[4,128,256]{2,1,0:T(8,128)(2,1)S(1)}, f32[8,128]{1,0:T(8,128)S(1)}) custom-call(bf16[128,4096]{1,0:T(8,128)(2,1)} %xs0.1, bf16[128,4096]{1,0:T(8,128)(2,1)} %xs1.1, bf16[256,1024]{1,0:T(8,128)(2,1)S(1)} %copy-done.5, ...), custom_call_target="tpu_custom_call" | custom-call | tf_op jit(solution)/shard_map/exchange/pallas_call | solution.py:298
  114.8 0.0 copy-done
  114.8 10.2 %update.1 = (f32[1024,1024]{1,0:T(8,128)}, bf16[1024,1024]{1,0:T(8,128)(2,1)}, f32[1024,1024]{1,0:T(8,128)}, bf16[1024,1024]{1,0:T(8,128)(2,1)}, f32[128,1024]{1...) custom-call(f32[8,128]{1,0:T(8,128)S(1)} %get-tuple-element.15.tot, ...), custom_call_target="tpu_custom_call" | custom-call | tf_op jit(solution)/shard_map/update/pallas_call | solution.py:346
Async XLA Ops:
  0.6 114.2 %copy-start = (bf16[1024,512]{1,0:T(8,128)(2,1)S(1)}, bf16[1024,512]{1,0:T(8,128)(2,1)}, u32[]{:S(2)}) copy-start(bf16[1024,512]{1,0:T(8,128)(2,1)} %fa0.3) | copy-start | bytes 3145732
  0.7 1.1 copy-start.1
  1.8 1.0 copy-start.2
  2.8 1.0 copy-start.3
  3.9 1.0 copy-start.4
  4.9 1.0 copy-start.5
  6.0 1.0 copy-start.6

commit v2 on v1

--- a/solution.py
+++ b/solution.py
@@ -26,7 +26,7 @@
     nfs, nrep,
     xs0, xs1, ct0, ct1, fa0, fa1, m10, m20, m11, m21,
     low0, low1, grad0, grad1, tot_out,
-    xin0, xin1, fb0, fb1, cv0, cv1, pb0, pb1, pt0, pt1, ra0, ra1, s0, s1, rb0, rb1,
+    xin0, xin1, fb0, fb1, cv0, cv1, pb0, pb1, pt0, pt1, ra0, ra1, u0, u1, s0, s1, rb0, rb1,
     gb0, gb1, lb0, lb1, mo, tb, acc,
     lsem, xsem, zsem, bsem, csem, asem, rsem, gsem, lzsem, lxsem, tsem, osem,
 ):
@@ -39,20 +39,19 @@
     xin, fb, cv, pb, pt, ra, sm, rb = (
         (xin0, xin1), (fb0, fb1), (cv0, cv1), (pb0, pb1), (pt0, pt1), (ra0, ra1), (s0, s1), (rb0, rb1),
     )
-    gb, lb = (gb0, gb1), (lb0, lb1)
+    gb, lb, ub = (gb0, gb1), (lb0, lb1), (u0, u1)
     rows = xs0.shape[0]
     depth, half = fb0.shape
     block = depth // nfs
     quarter = block // nrep
     chunk, width = rb0.shape[1:]
     zd = range(1, nfs)
-    xd = range(1, nrep)
+    px = r + 1 - 2 * lax.rem(r, 2)
+    py = lax.rem(r + 2, nrep)
+    pd = nrep - 1 - r
 
     def fs_at(d):
         return lax.rem(j + d + nfs, nfs)
-
-    def rep_at(e):
-        return lax.rem(r + e + nrep, nrep)
 
     def remote(src, dst, sems, idx, where):
         return pltpu.make_async_remote_copy(
@@ -63,30 +62,59 @@
     mine = pl.ds(pl.multiple_of(c * rows, rows), rows)
     half_cols = pl.ds(pl.multiple_of(c * half, half), half)
     own_rows = pl.ds(pl.multiple_of(j * block, block), block)
-    mcols = pl.ds(pl.multiple_of(r * width, width), width)
     local = {}
     for f in (0, 1):
         local["x", f] = pltpu.make_async_copy(xs[f], xin[f].at[mine], lsem.at[0, f])
         local["f", f] = pltpu.make_async_copy(fa[f].at[:, half_cols], fb[f].at[own_rows], lsem.at[1, f])
         local["c", f] = pltpu.make_async_copy(ct[f], cv[f], lsem.at[2, f])
-        local["1", f] = pltpu.make_async_copy(firsts[f].at[:, mcols], mo.at[f, 0], lsem.at[3, f])
-        local["2", f] = pltpu.make_async_copy(seconds[f].at[:, mcols], mo.at[f, 1], lsem.at[4, f])
+        local["1", f] = pltpu.make_async_copy(firsts[f], mo.at[f, 0], lsem.at[3, f])
+        local["2", f] = pltpu.make_async_copy(seconds[f], mo.at[f, 1], lsem.at[4, f])
 
     barrier = pltpu.get_barrier_semaphore()
     for d in zd:
         pl.semaphore_signal(barrier, inc=1, device_id={"fs": fs_at(d)}, device_id_type=MESH)
-    for e in xd:
-        pl.semaphore_signal(barrier, inc=1, device_id={"rep": rep_at(e)}, device_id_type=MESH)
+    for peer in (px, py):
+        pl.semaphore_signal(barrier, inc=1, device_id={"rep": peer}, device_id_type=MESH)
     pl.semaphore_signal(barrier, inc=1, device_id={"tp": mate}, device_id_type=MESH)
     for f in (0, 1):
         for k in ("x", "f", "c", "1", "2"):
             local[k, f].start()
-    pl.semaphore_wait(barrier, nfs + nrep - 1)
+    pl.semaphore_wait(barrier, nfs - 1 + 2 + 1)
 
     def frows(jj, rr):
         return pl.ds(pl.multiple_of(jj * block + rr * quarter, quarter), quarter)
 
     sends = []
+
+    def launch(cp):
+        cp.start()
+        sends.append(cp)
+
+    class Spread:
+        def __init__(self, view, sems, idx):
+            self.view, self.sems, self.idx = view, sems, idx
+
+        def copy(self, owner, part, k, peer):
+            view = self.view(owner, part)
+            return remote(view, view, self.sems, (*self.idx, k), {"rep": peer})
+
+        def give(self):
+            launch(self.copy(r, None, 0, px))
+            launch(self.copy(r, None, 1, py))
+
+        def relay(self):
+            self.copy(px, None, 0, px).wait_recv()
+            launch(self.copy(px, 0, 2, py))
+            self.copy(py, None, 1, py).wait_recv()
+            launch(self.copy(py, 1, 3, px))
+
+        def finish(self):
+            self.copy(pd, 0, 2, py).wait_recv()
+            self.copy(pd, 1, 3, px).wait_recv()
+
+    def lanes(size, part):
+        return pl.ds(0, size) if part is None else pl.ds(part * (size // 2), size // 2)
+
     zcp = {}
     for f in (0, 1):
         for d in zd:
@@ -107,14 +135,35 @@
         sends.append(cp)
         theirs = pl.ds(pl.multiple_of(mate * rows, rows), rows)
         xcp.append(remote(xs[f], xin[f].at[theirs], xsem, (f,), {"tp": mate}))
+    fspread = {}
+    last = None
     for f in (0, 1):
         for d in zd:
             zcp[f, d].wait_recv()
-            for e in xd:
-                view = fb[f].at[frows(fs_at(-d), r)]
-                cp = remote(view, view, bsem, (f, d - 1, e - 1), {"rep": rep_at(e)})
-                cp.start()
-                sends.append(cp)
+            item = Spread(
+                lambda rr, part, f=f, d=d: fb[f].at[frows(fs_at(-d), rr), lanes(half, part)],
+                bsem, (f, d - 1),
+            )
+            fspread[f, d] = item
+            item.give()
+            if last is not None:
+                last.relay()
+            last = item
+    last.relay()
+
+    def scatter(f, k):
+        owner, peer = ((px, px), (pd, px), (py, py), (pd, py))[k]
+        return remote(
+            pt[f].at[owner, :, :, lanes(width, k // 2)], ra[f].at[k], asem, (f, k), {"rep": peer}
+        )
+
+    def second(f, part):
+        return remote(ub[f].at[part], ra[f].at[4 + part], asem, (f, 4 + part), {"rep": (py, px)[part]})
+
+    def lowered(f, q):
+        cols = pl.ds(pl.multiple_of(q * width, width), width)
+        new_first, new_second = blend(gb[f][q].astype(F32), mo[f, 0, :, cols], mo[f, 1, :, cols])
+        lb[f][q, j] = (new_first / jnp.sqrt(new_second)).astype(BF16)
 
     kstep = min(512, depth)
     perhalf = half // chunk
@@ -124,9 +173,7 @@
             local[k, f].wait()
         xcp[f].wait_recv()
         for d in zd:
-            for e in xd:
-                view = fb[f].at[frows(fs_at(-d), rep_at(-e))]
-                remote(view, view, bsem, (f, d - 1, e - 1), {"rep": rep_at(e)}).wait_recv()
+            fspread[f, d].finish()
 
         acc[...] = jnp.zeros_like(acc)
 
@@ -156,20 +203,34 @@
         partials(c)
         remote(pb[f].at[mate], pb[f].at[mate], csem, (f,), {"tp": mate}).wait_recv()
         partials(mate)
-        for e in xd:
-            cp = remote(pt[f].at[rep_at(e)], ra[f].at[e - 1], asem, (f, e - 1), {"rep": rep_at(e)})
-            cp.start()
-            sends.append(cp)
-
-    for f in (0, 1):
-        for e in xd:
-            remote(pt[f].at[rep_at(e)], ra[f].at[e - 1], asem, (f, e - 1), {"rep": rep_at(e)}).wait_recv()
+        for k in (1, 3, 0, 2):
+            launch(scatter(f, k))
+
+    for f in (0, 1):
+        for k, owner, peer in ((1, py, py), (3, px, px)):
+            scatter(f, k).wait_recv()
+            part = k // 2
+            cols = lanes(width, part)
+
+            def fold(i, _, f=f, k=k, owner=owner, part=part, cols=cols):
+                total = pt[f][owner, i, :, cols].astype(F32) + ra[f][k, i].astype(F32)
+                ub[f][part, i] = total.astype(BF16)
+                return 0
+
+            lax.fori_loop(0, nfs, fold, 0)
+            launch(second(f, part))
+    for f in (0, 1):
+        scatter(f, 0).wait_recv()
+        scatter(f, 2).wait_recv()
+        second(f, 0).wait_recv()
+        second(f, 1).wait_recv()
 
         def add(i, _, f=f):
-            total = pt[f][r, i].astype(F32)
-            for e in xd:
-                total += ra[f][e - 1, i].astype(F32)
-            sm[f][i] = total.astype(BF16)
+            for part in (0, 1):
+                cols = lanes(width, part)
+                total = pt[f][r, i, :, cols].astype(F32) + ra[f][2 * part, i].astype(F32)
+                total += ra[f][4 + part, i].astype(F32)
+                sm[f][i, :, cols] = total.astype(BF16)
             return 0
 
         lax.fori_loop(0, nfs, add, 0)
@@ -178,6 +239,7 @@
             cp.start()
             sends.append(cp)
 
+    outs, gspread = [], []
     for f in (0, 1):
         local["1", f].wait()
         local["2", f].wait()
@@ -186,40 +248,39 @@
         total = sm[f][j].astype(F32)
         for d in zd:
             total += rb[f][d - 1].astype(F32)
-        kept = total.astype(BF16)
-        gb[f][r] = kept
-        new_first, new_second = blend(kept.astype(F32), mo[f, 0], mo[f, 1])
-        lb[f][r, j] = (new_first / jnp.sqrt(new_second)).astype(BF16)
+        gb[f][r] = total.astype(BF16)
+        lowered(f, r)
         for d in zd:
             view = lb[f].at[r, j]
-            cp = remote(view, view, lzsem, (f, d - 1), {"fs": fs_at(d)})
-            cp.start()
-            sends.append(cp)
-        for e in xd:
-            view = lb[f].at[r, j]
-            cp = remote(view, view, lxsem, (f, 0, e - 1), {"rep": rep_at(e)})
-            cp.start()
-            sends.append(cp)
-
+            launch(remote(view, view, lzsem, (f, d - 1), {"fs": fs_at(d)}))
+        gspread.append(Spread(lambda rr, part, f=f: gb[f].at[rr, :, lanes(width, part)], gsem, (f,)))
+        gspread[f].give()
+    for f in (0, 1):
+        gspread[f].relay()
+
+    lspread = []
     for f in (0, 1):
         for d in zd:
             view = lb[f].at[r, fs_at(-d)]
             remote(view, view, lzsem, (f, d - 1), {"fs": fs_at(d)}).wait_recv()
-            for e in xd:
-                cp = remote(view, view, lxsem, (f, d, e - 1), {"rep": rep_at(e)})
-                cp.start()
-                sends.append(cp)
-    for f in (0, 1):
-        for e in xd:
-            cp = remote(gb[f].at[r], gb[f].at[r], gsem, (f, e - 1), {"rep": rep_at(e)})
-            cp.start()
-            sends.append(cp)
-    for f in (0, 1):
-        for d in range(nfs):
-            for e in xd:
-                view = lb[f].at[rep_at(-e), fs_at(-d)]
-                remote(view, view, lxsem, (f, d, e - 1), {"rep": rep_at(e)}).wait_recv()
-    outs = []
+            item = Spread(
+                lambda rr, part, f=f, d=d: lb[f].at[rr, fs_at(-d), :, lanes(width, part)],
+                lxsem, (f, d - 1),
+            )
+            item.give()
+            if lspread:
+                lspread[-1].relay()
+            lspread.append(item)
+    lspread[-1].relay()
+    for f in (0, 1):
+        gspread[f].finish()
+        cp = pltpu.make_async_copy(gb[f], grads[f], osem.at[f, 1])
+        cp.start()
+        outs.append(cp)
+        for q in (px, py, pd):
+            lowered(f, q)
+    for item in lspread:
+        item.finish()
     for f in (0, 1):
         cp = pltpu.make_async_copy(lb[f], lows[f], osem.at[f, 0])
         cp.start()
@@ -239,13 +300,6 @@
     cp = remote(tb.at[c], tb.at[c], tsem, (), {"tp": mate})
     cp.start()
     sends.append(cp)
-    for f in (0, 1):
-        for e in xd:
-            view = gb[f].at[rep_at(-e)]
-            remote(view, view, gsem, (f, e - 1), {"rep": rep_at(e)}).wait_recv()
-        cp = pltpu.make_async_copy(gb[f], grads[f], osem.at[f, 1])
-        cp.start()
-        outs.append(cp)
     remote(tb.at[mate], tb.at[mate], tsem, (), {"tp": mate}).wait_recv()
     tot_out[...] = tb[0] + tb[1]
     for cp in outs:
@@ -279,13 +333,15 @@
 
 
 def shards(nfs, nrep, ntp, xs0, xs1, ct0, ct1, fa0, fa1, w0, w1, m10, m20, m11, m21):
+    assert nrep == 4
     rows, depth = xs0.shape
     tokens, chans = ct0.shape
     rank = fa0.shape[1]
     half = rank // ntp
     chunk = rank // nfs
     width = chans // nrep
-    hbm = pl.BlockSpec(memory_space=pl.ANY)
+    hbm = pl.BlockSpec(memory_space=pltpu.HBM)
+    free = pl.BlockSpec(memory_space=pl.ANY)
     vmem = pl.BlockSpec(memory_space=pltpu.VMEM)
     sds = jax.ShapeDtypeStruct
 
@@ -301,34 +357,35 @@
         + [sds((nrep, chunk, width), BF16)] * 2
         + [sds((8, 128), F32)],
         in_specs=[hbm] * 10,
-        out_specs=[hbm] * 4 + [vmem],
+        out_specs=[free] * 4 + [vmem],
         scratch_shapes=twice((tokens, depth))
         + twice((depth, half))
         + twice((tokens, chans))
         + twice((ntp, half, tokens))
         + twice((nrep, nfs, chunk, width))
-        + twice((nrep - 1, nfs, chunk, width))
+        + twice((6, nfs, chunk, width // 2))
+        + twice((2, nfs, chunk, width // 2))
         + twice((nfs, chunk, width))
         + twice((nfs - 1, chunk, width))
         + twice((nrep, chunk, width))
         + twice((nrep, nfs, chunk, width))
-        + [pltpu.VMEM((2, 2, chunk, width), F32), pltpu.VMEM((ntp, 8, 128), F32), pltpu.VMEM((tokens, half), F32)]
+        + [pltpu.VMEM((2, 2, chunk, chans), F32), pltpu.VMEM((ntp, 8, 128), F32), pltpu.VMEM((tokens, half), F32)]
         + [
             sems(5, 2),
             sems(2, 2),
             sems(2, 2, nfs - 1),
-            sems(2, 2, nfs - 1, nrep - 1),
+            sems(2, 2, nfs - 1, 4),
             sems(2, 2),
-            sems(2, 2, nrep - 1),
+            sems(2, 2, 6),
             sems(2, 2, nfs - 1),
-            sems(2, 2, nrep - 1),
+            sems(2, 2, 4),
             sems(2, 2, nfs - 1),
-            sems(2, 2, nfs, nrep - 1),
+            sems(2, 2, nfs - 1, 4),
             sems(2),
             sems(2, 2),
         ],
         compiler_params=pltpu.CompilerParams(
-            collective_id=0, has_side_effects=True, vmem_limit_bytes=48 * 1024 * 1024
+            collective_id=0, has_side_effects=True, vmem_limit_bytes=62 * 1024 * 1024
         ),
         name="exchange",
     )(xs0, xs1, ct0, ct1, fa0, fa1, m10, m20, m11, m21)
@@ -353,7 +410,7 @@
         in_specs=[pl.BlockSpec((8, 128), lambda q: (0, 0)), one, one, gsp, gsp, whole, whole, wcol, wrow]
         + [msp] * 4,
         out_specs=[wcol, wcol, wrow, wrow] + [msp] * 6,
-        compiler_params=pltpu.CompilerParams(vmem_limit_bytes=48 * 1024 * 1024),
+        compiler_params=pltpu.CompilerParams(vmem_limit_bytes=60 * 1024 * 1024),
         name="update",
     )(tot, low0, low1, grad0, grad1, fa0, fa1, w0, w1, m10, m20, m11, m21)
     return nw0, cw0, nw1, cw1, n10, n20, n11, n21, st0, st1

time: 125 us -> 116 us (0.928)
  the two profiles are of different devices: /device:TPU:16 before, /device:TPU:25 now
where the time goes in v2:
time: 116 us; the launch traced here: 115 us
  Pallas kernels  115 us (99%)
    pallas_call x1, Pallas kernels, shards(): pl.pallas_call(functools.partial(exchange_kernel, nfs, nrep), out_shape=[...  102 us
    pallas_call x1, Pallas kernels, shards(): pl.pallas_call(functools.partial(update_kernel, 2.0 * rank * chans * ntp)...  12.5 us

profile of v2, /device:TPU:25, one launch (start us, length us, event | category | flops | bytes accessed | tf_op | source)
XLA Modules:
  0.0 115.4 jit_solution(10860448422133693950)
XLA Ops:
  0.6 102.3 %exchange.1 = (bf16[4,4,128,256]{3,2,1,0:T(8,128)(2,1)}, bf16[4,4,128,256]{3,2,1,0:T(8,128)(2,1)}, bf16[4,128,256]{2,1,0:T(8,128)(2,1)}, bf16[4,128,256]{2,1,0:T(8,128)(2,1)}, f32[8,128]{1,0:T(8,128)}) custom-call(bf16[128,4096]{1,0:T(8,128)(2,1)} %xs0.1, bf16[128,4096]{1,0:T(8,128)(2,1)} %xs1.1, bf16[256,1024]{1,0:T(8,128)(2,1)} %ct0.1, ...), custom_call_target="tpu_custom_call" | custom-call | tf_op jit(solution)/shard_map/exchange/pallas_call | solution.py:354
  102.9 12.5 %update.1 = (f32[1024,1024]{1,0:T(8,128)}, bf16[1024,1024]{1,0:T(8,128)(2,1)}, f32[1024,1024]{1,0:T(8,128)}, bf16[1024,1024]{1,0:T(8,128)(2,1)}, f32[128,1024]{1...) custom-call(f32[8,128]{1,0:T(8,128)} %get-tuple-element.15.tot, ...), custom_call_target="tpu_custom_call" | custom-call | tf_op jit(solution)/shard_map/update/pallas_call | solution.py:403

commit v3 on v2

--- a/solution.py
+++ b/solution.py
@@ -51,7 +51,11 @@
     pd = nrep - 1 - r
 
     def fs_at(d):
-        return lax.rem(j + d + nfs, nfs)
+        at = j
+        for bit in (1 << i for i in range(d.bit_length())):
+            if d & bit:
+                at = at + bit - 2 * bit * lax.rem(lax.div(j, bit), 2)
+        return at
 
     def remote(src, dst, sems, idx, where):
         return pltpu.make_async_remote_copy(
@@ -126,7 +130,7 @@
             sends.append(cp)
             zcp[f, d] = remote(
                 fa[f].at[pl.ds(pl.multiple_of(r * quarter, quarter), quarter), half_cols],
-                fb[f].at[frows(fs_at(-d), r)], zsem, (f, d - 1), {"fs": fs_at(d)},
+                fb[f].at[frows(fs_at(d), r)], zsem, (f, d - 1), {"fs": fs_at(d)},
             )
     xcp = []
     for f in (0, 1):
@@ -135,13 +139,80 @@
         sends.append(cp)
         theirs = pl.ds(pl.multiple_of(mate * rows, rows), rows)
         xcp.append(remote(xs[f], xin[f].at[theirs], xsem, (f,), {"tp": mate}))
+    def scatter(f, k):
+        owner, peer = ((px, px), (pd, px), (py, py), (pd, py))[k]
+        return remote(
+            pt[f].at[owner, :, :, lanes(width, k // 2)], ra[f].at[k], asem, (f, k), {"rep": peer}
+        )
+
+    def second(f, part):
+        return remote(ub[f].at[part], ra[f].at[4 + part], asem, (f, 4 + part), {"rep": (py, px)[part]})
+
+    def halve(f):
+        for k, owner in ((1, py), (3, px)):
+            scatter(f, k).wait_recv()
+            part = k // 2
+            cols = lanes(width, part)
+
+            def fold(i, _, k=k, owner=owner, part=part, cols=cols):
+                total = pt[f][owner, i, :, cols].astype(F32) + ra[f][k, i].astype(F32)
+                ub[f][part, i] = total.astype(BF16)
+                return 0
+
+            lax.fori_loop(0, nfs, fold, 0)
+            launch(second(f, part))
+
+    def lowered(f, q):
+        cols = pl.ds(pl.multiple_of(q * width, width), width)
+        new_first, new_second = blend(gb[f][q].astype(F32), mo[f, 0, :, cols], mo[f, 1, :, cols])
+        lb[f][q, j] = (new_first / jnp.sqrt(new_second)).astype(BF16)
+
+    kstep = min(512, depth)
+    perhalf = half // chunk
+
     fspread = {}
+
+    def compute(f):
+        for k in ("x", "f", "c"):
+            local[k, f].wait()
+        xcp[f].wait_recv()
+        for d in zd:
+            fspread[f, d].finish()
+
+        acc[...] = jnp.zeros_like(acc)
+
+        def project(k, _, f=f):
+            ks = pl.ds(pl.multiple_of(k * kstep, kstep), kstep)
+            acc[...] += jnp.dot(xin[f][:, ks], fb[f][ks, :], preferred_element_type=F32)
+            return 0
+
+        lax.fori_loop(0, depth // kstep, project, 0)
+        pb[f][c] = jnp.transpose(acc[...]).astype(BF16)
+        cp = remote(pb[f].at[c], pb[f].at[c], csem, (f,), {"tp": mate})
+        cp.start()
+        sends.append(cp)
+
+        def partials(h, f=f):
+            left = pb[f][h]
+
+            def piece(q, _):
+                cols = pl.ds(pl.multiple_of(q * width, width), width)
+                out = jnp.dot(left, cv[f][:, cols], preferred_element_type=F32)
+                for i in range(perhalf):
+                    pt[f][q, h * perhalf + i] = out[i * chunk:(i + 1) * chunk].astype(BF16)
+                return 0
+
+            lax.fori_loop(0, nrep, piece, 0)
+
+        partials(c)
+        remote(pb[f].at[mate], pb[f].at[mate], csem, (f,), {"tp": mate}).wait_recv()
+        partials(mate)
     last = None
     for f in (0, 1):
         for d in zd:
             zcp[f, d].wait_recv()
             item = Spread(
-                lambda rr, part, f=f, d=d: fb[f].at[frows(fs_at(-d), rr), lanes(half, part)],
+                lambda rr, part, f=f, d=d: fb[f].at[frows(fs_at(d), rr), lanes(half, part)],
                 bsem, (f, d - 1),
             )
             fspread[f, d] = item
@@ -149,76 +220,18 @@
             if last is not None:
                 last.relay()
             last = item
+    compute(0)
     last.relay()
-
-    def scatter(f, k):
-        owner, peer = ((px, px), (pd, px), (py, py), (pd, py))[k]
-        return remote(
-            pt[f].at[owner, :, :, lanes(width, k // 2)], ra[f].at[k], asem, (f, k), {"rep": peer}
-        )
-
-    def second(f, part):
-        return remote(ub[f].at[part], ra[f].at[4 + part], asem, (f, 4 + part), {"rep": (py, px)[part]})
-
-    def lowered(f, q):
-        cols = pl.ds(pl.multiple_of(q * width, width), width)
-        new_first, new_second = blend(gb[f][q].astype(F32), mo[f, 0, :, cols], mo[f, 1, :, cols])
-        lb[f][q, j] = (new_first / jnp.sqrt(new_second)).astype(BF16)
-
-    kstep = min(512, depth)
-    perhalf = half // chunk
-
-    for f in (0, 1):
-        for k in ("x", "f", "c"):
-            local[k, f].wait()
-        xcp[f].wait_recv()
-        for d in zd:
-            fspread[f, d].finish()
-
-        acc[...] = jnp.zeros_like(acc)
-
-        def project(k, _, f=f):
-            ks = pl.ds(pl.multiple_of(k * kstep, kstep), kstep)
-            acc[...] += jnp.dot(xin[f][:, ks], fb[f][ks, :], preferred_element_type=F32)
-            return 0
-
-        lax.fori_loop(0, depth // kstep, project, 0)
-        pb[f][c] = jnp.transpose(acc[...]).astype(BF16)
-        cp = remote(pb[f].at[c], pb[f].at[c], csem, (f,), {"tp": mate})
-        cp.start()
-        sends.append(cp)
-
-        def partials(h, f=f):
-            left = pb[f][h]
-
-            def piece(q, _):
-                cols = pl.ds(pl.multiple_of(q * width, width), width)
-                out = jnp.dot(left, cv[f][:, cols], preferred_element_type=F32)
-                for i in range(perhalf):
-                    pt[f][q, h * perhalf + i] = out[i * chunk:(i + 1) * chunk].astype(BF16)
-                return 0
-
-            lax.fori_loop(0, nrep, piece, 0)
-
-        partials(c)
-        remote(pb[f].at[mate], pb[f].at[mate], csem, (f,), {"tp": mate}).wait_recv()
-        partials(mate)
-        for k in (1, 3, 0, 2):
-            launch(scatter(f, k))
-
-    for f in (0, 1):
-        for k, owner, peer in ((1, py, py), (3, px, px)):
-            scatter(f, k).wait_recv()
-            part = k // 2
-            cols = lanes(width, part)
-
-            def fold(i, _, f=f, k=k, owner=owner, part=part, cols=cols):
-                total = pt[f][owner, i, :, cols].astype(F32) + ra[f][k, i].astype(F32)
-                ub[f][part, i] = total.astype(BF16)
-                return 0
-
-            lax.fori_loop(0, nfs, fold, 0)
-            launch(second(f, part))
+    for k in (1, 3, 0, 2):
+        launch(scatter(0, k))
+    compute(1)
+    for k in (1, 3):
+        launch(scatter(1, k))
+    halve(0)
+    for k in (0, 2):
+        launch(scatter(1, k))
+    halve(1)
+
     for f in (0, 1):
         scatter(f, 0).wait_recv()
         scatter(f, 2).wait_recv()
@@ -261,10 +274,10 @@
     lspread = []
     for f in (0, 1):
         for d in zd:
-            view = lb[f].at[r, fs_at(-d)]
+            view = lb[f].at[r, fs_at(d)]
             remote(view, view, lzsem, (f, d - 1), {"fs": fs_at(d)}).wait_recv()
             item = Spread(
-                lambda rr, part, f=f, d=d: lb[f].at[rr, fs_at(-d), :, lanes(width, part)],
+                lambda rr, part, f=f, d=d: lb[f].at[rr, fs_at(d), :, lanes(width, part)],
                 lxsem, (f, d - 1),
             )
             item.give()
@@ -333,7 +346,7 @@
 
 
 def shards(nfs, nrep, ntp, xs0, xs1, ct0, ct1, fa0, fa1, w0, w1, m10, m20, m11, m21):
-    assert nrep == 4
+    assert nrep == 4 and nfs & (nfs - 1) == 0
     rows, depth = xs0.shape
     tokens, chans = ct0.shape
     rank = fa0.shape[1]

time: 116 us -> 109 us (0.940)
  the two profiles are of different devices: /device:TPU:25 before, /device:TPU:0 now
where the time goes in v3:
time: 109 us; the launch traced here: 107 us
  Pallas kernels  107 us (98%)
    pallas_call x1, Pallas kernels, shards(): pl.pallas_call(functools.partial(exchange_kernel, nfs, nrep), out_shape=[...  94 us
    pallas_call x1, Pallas kernels, shards(): pl.pallas_call(functools.partial(update_kernel, 2.0 * rank * chans * ntp)...  12.5 us

profile of v3, /device:TPU:0, one launch (start us, length us, event | category | flops | bytes accessed | tf_op | source)
XLA Modules:
  0.0 107.2 jit_solution(15563639314659340012)
XLA Ops:
  0.6 94.0 %exchange.1 = (bf16[4,4,128,256]{3,2,1,0:T(8,128)(2,1)}, bf16[4,4,128,256]{3,2,1,0:T(8,128)(2,1)}, bf16[4,128,256]{2,1,0:T(8,128)(2,1)}, bf16[4,128,256]{2,1,0:T(8,128)(2,1)}, f32[8,128]{1,0:T(8,128)}) custom-call(bf16[128,4096]{1,0:T(8,128)(2,1)} %xs0.1, bf16[128,4096]{1,0:T(8,128)(2,1)} %xs1.1, bf16[256,1024]{1,0:T(8,128)(2,1)} %ct0.1, ...), custom_call_target="tpu_custom_call" | custom-call | tf_op jit(solution)/shard_map/exchange/pallas_call | solution.py:367
  94.7 12.5 %update.1 = (f32[1024,1024]{1,0:T(8,128)}, bf16[1024,1024]{1,0:T(8,128)(2,1)}, f32[1024,1024]{1,0:T(8,128)}, bf16[1024,1024]{1,0:T(8,128)(2,1)}, f32[128,1024]{1...) custom-call(f32[8,128]{1,0:T(8,128)} %get-tuple-element.15.tot, ...), custom_call_target="tpu_custom_call" | custom-call | tf_op jit(solution)/shard_map/update/pallas_call | solution.py:416
